TPU v7x, 32 devices: a whole 2x2x4 slice. The times are simulated.
32 devices in a mesh: fs: 4 (over z), rep: 4 (over y, x), tp: 2 (over core).
Axes of the slice: x: 2, y: 2, z: 4, core: 2. Of those that a mesh axis runs over, the one named last changes fastest.
Arguments:
- saved_latent: bfloat16 [12288, 2048], P(('fs', 'rep')), may hold values from -6 to 6
- query_cotangent: bfloat16 [12288, 3072], P(('fs', 'rep'), 'tp'), may hold values from -6 to 6
- mix_cotangent: bfloat16 [12288, 4096], P(('fs', 'rep')), may hold values from -6 to 6
- head_outputs: bfloat16 [12288, 2048], P(('fs', 'rep'), 'tp'), may hold values from -6 to 6
- query_weight: float32 [2048, 3072], P('fs', 'tp'), may hold values from -0.125 to 0.125
- out_weight: float32 [4096, 2048], P('fs', 'tp'), may hold values from -0.125 to 0.125
- query_basis: bfloat16 [2048, 256], replicated, may hold values from -0.125 to 0.125
- out_basis: bfloat16 [4096, 256], replicated, may hold values from -0.09375 to 0.09375
- query_mean: float32 [256, 3072], P('fs', 'tp'), may hold values from -3 to 3
- query_var: float32 [256, 3072], P('fs', 'tp'), may hold values from 0.1 to 1
- out_mean: float32 [256, 2048], P('fs', 'tp'), may hold values from -3 to 3
- out_var: float32 [256, 2048], P('fs', 'tp'), may hold values from 0.1 to 1
Outputs:
- query_step: float32 [2048, 3072], P('fs', 'tp')
- out_step: float32 [4096, 2048], P('fs', 'tp')
- query_copy: bfloat16 [2048, 3072], P('fs', 'tp')
- out_copy: bfloat16 [4096, 2048], P('fs', 'tp')
All inputs are finite; a program needn't handle non-finite values.
Results may differ from a plain program's by a relative error of at most 0.001.
Values sent between devices are 32-bit elements; how exact they have to be, the bound alone decides.
A program may use at most 128 MiB of HBM per device.

v0:
```python
import jax
import jax.numpy as jnp
from jax import lax
from jax.sharding import PartitionSpec as P


def token_sum(left, right):
    return lax.dot_general(
        left, right, (((0,), (0,)), ((), ())), preferred_element_type=jnp.float32
    )


def project(basis, grad):
    return lax.dot_general(
        basis.astype(jnp.float32), grad, (((0,), (0,)), ((), ())), precision=lax.Precision.HIGHEST
    )


def moment_direction(proj, scale, mean, var):
    scaled = scale * proj
    new_mean = 0.8 * mean + 0.2 * scaled
    new_var = 0.9 * var + 0.1 * scaled * scaled
    return new_mean / jnp.sqrt(new_var)


def on_device(
    saved_latent,
    query_cotangent,
    mix_cotangent,
    head_outputs,
    query_weight,
    out_weight,
    query_basis,
    out_basis,
    query_mean,
    query_var,
    out_mean,
    out_var,
):
    query_rows = query_weight.shape[0]
    out_rows = out_weight.shape[0]
    position = lax.axis_index("fs")
    query_local = lax.dynamic_slice_in_dim(query_basis, position * query_rows, query_rows, 0)
    out_local = lax.dynamic_slice_in_dim(out_basis, position * out_rows, out_rows, 0)
    query_early = project(query_basis, token_sum(saved_latent, query_cotangent))
    out_early = project(out_basis, token_sum(mix_cotangent, head_outputs))
    query_shard, out_shard = (
        lax.psum_scatter(query_early, "fs", scatter_dimension=0, tiled=True),
        lax.psum_scatter(out_early, "fs", scatter_dimension=0, tiled=True),
    )
    query_proj, out_proj = lax.psum((query_shard, out_shard), "rep")
    query_squares, out_squares = lax.psum(
        (jnp.sum(query_proj * query_proj), jnp.sum(out_proj * out_proj)), ("fs", "tp")
    )
    spread = lax.axis_size("fs") * lax.axis_size("tp")
    query_count = float(query_proj.shape[0] * query_proj.shape[1] * spread)
    out_count = float(out_proj.shape[0] * out_proj.shape[1] * spread)
    query_scale = 1.0 / jnp.maximum(jnp.sqrt(query_squares / query_count), 1.0)
    out_scale = 1.0 / jnp.maximum(jnp.sqrt(out_squares / out_count), 1.0)
    query_dir = moment_direction(query_proj, query_scale, query_mean, query_var)
    out_dir = moment_direction(out_proj, out_scale, out_mean, out_var)
    query_left = query_local.astype(jnp.float32)
    out_left = out_local.astype(jnp.float32)
    query_step = jnp.dot(
        query_left,
        lax.all_gather(query_dir, "fs", axis=0, tiled=True),
        precision=lax.Precision.HIGHEST,
    )
    out_step = jnp.dot(
        out_left, lax.all_gather(out_dir, "fs", axis=0, tiled=True), precision=lax.Precision.HIGHEST
    )
    query_copy = (query_weight - 0.05 * query_step).astype(jnp.bfloat16)
    out_copy = (out_weight - 0.05 * out_step).astype(jnp.bfloat16)
    return (query_step, out_step, query_copy, out_copy)


def solution(mesh):
    placed = (
        P(("fs", "rep"), None),
        P(("fs", "rep"), "tp"),
        P(("fs", "rep"), None),
        P(("fs", "rep"), "tp"),
        P("fs", "tp"),
        P("fs", "tp"),
        P(),
        P(),
        P("fs", "tp"),
        P("fs", "tp"),
        P("fs", "tp"),
        P("fs", "tp"),
    )
    return jax.shard_map(
        on_device,
        mesh=mesh,
        in_specs=placed,
        out_specs=(P("fs", "tp"), P("fs", "tp"), P("fs", "tp"), P("fs", "tp")),
        check_vma=False,
    )
```

profile of v0, /device:TPU:0, one launch (start us, length us, event | category | flops | bytes accessed | tf_op | source)
XLA Modules:
  0.0 259.1 jit_solution(1730076010502316369)
XLA Ops:
  7.2 0.0 copy-start
  7.2 0.0 reduce-scatter.9.cloned.1.call-start
  7.2 0.0 copy-start.2
  7.2 9.9 %fusion.13 = f32[4096,1024]{1,0:T(8,128)S(1)} fusion(bf16[768,4096]{1,0:T(8,128)(2,1)} %param.14, bf16[768,1024]{1,0:T(8,128)(2,1)} %param.15), kind=kOutput, calls=%fused_computation.21 | convolution fusion | flops 6442450944 | bytes 24641536 | tf_op jit(solution)/shard_map/dot_general | solution.py:8
  17.1 0.0 copy-done.2
  17.1 24.0 %convolution_bitcast_fusion.1 = f32[256,1024]{0,1:T(8,128)} fusion(f32[4096,1024]{1,0:T(8,128)S(1)} %fusion.13, bf16[4096,256]{1,0:T(8,128)(2,1)S(1)} %copy-done.2), kind=kOutput, calls=%fused_computation.3 | convolution fusion | flops 12884901888 | bytes 19922944 | tf_op jit(solution)/shard_map/dot_general | solution.py:14
  41.2 2.5 copy.30
  43.7 0.0 reduce-scatter.9.cloned.1.call-update
  43.7 0.0 reduce-scatter.7.cloned.1.call-start
  43.8 0.0 copy-done
  43.8 0.0 copy-start.3
  43.8 7.0 %fusion.12 = f32[2048,1536]{1,0:T(8,128)S(1)} fusion(bf16[768,2048]{1,0:T(8,128)(2,1)S(1)} %copy-done, bf16[768,1536]{1,0:T(8,128)(2,1)} %param.13), kind=kOutput, calls=%fused_computation.20 | convolution fusion | flops 4831838208 | bytes 18087936 | tf_op jit(solution)/shard_map/dot_general | solution.py:8
  50.8 0.0 copy-done.3
  50.8 10.6 %convolution_bitcast_fusion = f32[256,1536]{0,1:T(8,128)S(1)} fusion(f32[2048,1536]{1,0:T(8,128)S(1)} %fusion.12, bf16[2048,256]{1,0:T(8,128)(2,1)S(1)} %copy-done.3), kind=kOutput, calls=%fused_computation.2 | convolution fusion | flops 9663676416 | bytes 15204352 | tf_op jit(solution)/shard_map/dot_general | solution.py:14
  61.4 0.0 copy-start.6
  61.4 0.0 copy-start.7
  61.4 0.0 copy-start.4
  61.5 0.0 copy-start.5
  61.5 1.6 copy.28
  63.1 0.0 reduce-scatter.7.cloned.1.call-update
  63.1 0.0 all-reduce.4.cloned.1.call-start
  63.2 10.7 %reduce-scatter.9.cloned.1.call-done = f32[64,1024]{1,0:T(8,128)} async-done(((f32[256,1024]{1,0:T(8,128)}), f32[64,1024]{1,0:T(8,128)}) %reduce-scatter.9.cloned.1.call-update) | async-done | bytes 262160 | tf_op jit(solution)/shard_map/reduce_scatter | solution.py:49
  73.9 36.9 %reduce-scatter.7.cloned.1.call-done = f32[64,1536]{1,0:T(8,128)} async-done(((f32[256,1536]{1,0:T(8,128)}), f32[64,1536]{1,0:T(8,128)}) %reduce-scatter.7.cloned.1.call-update) | async-done | bytes 393232 | tf_op jit(solution)/shard_map/reduce_scatter | solution.py:48
  110.7 0.0 all-reduce.4.cloned.1.call-update
  110.7 0.0 all-gather.5.cloned.1.call-start
  110.8 48.7 %all-reduce.4.cloned.1.call-done = (f32[64,1536]{1,0:T(8,128)}, f32[64,1024]{1,0:T(8,128)}) async-done(((f32[64,1536]{1,0:T(8,128)}, f32[64,1024]{1,0:T(8,128)}), (f32[64,1536]{1,0:T(8,128)}, f32[64,1024]{1,0:T(8,128)})) %all-reduce.4.cloned.1.call-update) | async-done | bytes 655376 | tf_op jit(solution)/shard_map/psum | solution.py:51
  159.5 1.7 multiply_reduce_fusion
  161.2 1.6 multiply_reduce_fusion.1
  162.8 16.9 %all-reduce = (f32[]{:T(128)}, f32[]{:T(128)}) all-reduce(f32[]{:T(128)} %multiply_reduce_fusion, f32[]{:T(128)} %multiply_reduce_fusion.1), channel_id=1, replica_groups=mesh['fs'=4,'rep'=4,'tp'=2] {'fs','tp'}, use_global_device_ids=true, to_apply=%region_3.0 | all-reduce | flops 2 | bytes 16 | tf_op jit(solution)/shard_map/psum | solution.py:52
  180.4 0.0 copy-done.6
  180.4 0.0 copy-done.7
  180.5 1.7 fusion.7
  182.2 0.0 all-gather.5.cloned.1.call-update
  182.2 0.0 all-gather.3.cloned.1.call-start
  183.0 0.0 copy-done.4
  183.0 0.0 copy-done.5
  183.0 1.9 fusion.4
  184.9 0.0 all-gather.3.cloned.1.call-update
  184.9 22.7 %all-gather.5.cloned.1.call-done = f32[256,1024]{1,0:T(8,128)} async-done(((f32[64,1024]{1,0:T(8,128)}), f32[256,1024]{1,0:T(8,128)}) %all-gather.5.cloned.1.call-update) | async-done | bytes 1048592 | tf_op jit(solution)/shard_map/all_gather | solution.py:70
  207.6 0.0 copy-start.1
  207.6 7.6 %subtract_convert_fusion = (bf16[1024,1024]{1,0:T(8,128)(2,1)}, f32[1024,1024]{1,0:T(8,128)}) fusion(f32[1024,1024]{1,0:T(8,128)} %param.17, f32[256,1024]{1,0:T(8,128)} %all-gather.5.cloned.1.call-done, bf16[4096,256]{1,0:T(8,128)(2,1)} %param.19, s32[]{:T(128)S(6)} %select_n.7), kind=kOutput, calls=%fused_computation | convolution fusion | flops 3224371200 | bytes 12058628 | tf_op jit(solution)/shard_map/dot_general | solution.py:69
  215.2 30.8 %all-gather.3.cloned.1.call-done = f32[256,1536]{1,0:T(8,128)} async-done(((f32[64,1536]{1,0:T(8,128)}), f32[256,1536]{1,0:T(8,128)}) %all-gather.3.cloned.1.call-update) | async-done | bytes 1572880 | tf_op jit(solution)/shard_map/all_gather | solution.py:66
  246.0 6.3 %subtract_convert_fusion.1 = (bf16[512,1536]{1,0:T(8,128)(2,1)}, f32[512,1536]{1,0:T(8,128)}) fusion(f32[512,1536]{1,0:T(8,128)} %param.16, f32[256,1536]{1,0:T(8,128)} %all-gather.3.cloned.1.call-done, bf16[2048,256]{1,0:T(8,128)(2,1)} %param.18, s32[]{:T(128)S(6)} %select_n.6), kind=kOutput, calls=%fused_computation.1 | convolution fusion | flops 2418278400 | bytes 9699332 | tf_op jit(solution)/shard_map/dot_general | solution.py:64
  252.3 0.0 copy-done.1
Async XLA Ops:
  7.2 36.6 %copy-start = (bf16[768,2048]{1,0:T(8,128)(2,1)S(1)}, bf16[768,2048]{1,0:T(8,128)(2,1)}, u32[]{:S(2)}) copy-start(bf16[768,2048]{1,0:T(8,128)(2,1)} %param.12) | copy-start | bytes 9437188
  7.2 66.7 %reduce-scatter.9.cloned.1.call-start = ((), (), s32[]{:S(2)}) async-start(), calls=%async_computation.5 | async-start | bytes 1310720 | tf_op jit(solution)/shard_map/reduce_scatter | solution.py:49
  7.2 9.9 %copy-start.2 = (bf16[4096,256]{1,0:T(8,128)(2,1)S(1)}, bf16[4096,256]{1,0:T(8,128)(2,1)}, u32[]{:S(2)}) copy-start(bf16[4096,256]{1,0:T(8,128)(2,1)} %param.19) | copy-start | bytes 6291460
  43.7 67.0 %reduce-scatter.7.cloned.1.call-start = ((), (), s32[]{:S(2)}) async-start(), calls=%async_computation.4 | async-start | bytes 1966080 | tf_op jit(solution)/shard_map/reduce_scatter | solution.py:48
  43.8 7.1 %copy-start.3 = (bf16[2048,256]{1,0:T(8,128)(2,1)S(1)}, bf16[2048,256]{1,0:T(8,128)(2,1)}, u32[]{:S(2)}) copy-start(bf16[2048,256]{1,0:T(8,128)(2,1)} %param.18) | copy-start | bytes 3145732
  61.4 119.0 %copy-start.6 = (f32[64,1024]{1,0:T(8,128)S(1)}, f32[64,1024]{1,0:T(8,128)}, u32[]{:S(2)}) copy-start(f32[64,1024]{1,0:T(8,128)} %param.23) | copy-start | bytes 786436
  61.4 119.0 %copy-start.7 = (f32[64,1024]{1,0:T(8,128)S(1)}, f32[64,1024]{1,0:T(8,128)}, u32[]{:S(2)}) copy-start(f32[64,1024]{1,0:T(8,128)} %param.22) | copy-start | bytes 786436
  61.4 121.6 %copy-start.4 = (f32[64,1536]{1,0:T(8,128)S(1)}, f32[64,1536]{1,0:T(8,128)}, u32[]{:S(2)}) copy-start(f32[64,1536]{1,0:T(8,128)} %param.21) | copy-start | bytes 1179652
  61.5 121.6 %copy-start.5 = (f32[64,1536]{1,0:T(8,128)S(1)}, f32[64,1536]{1,0:T(8,128)}, u32[]{:S(2)}) copy-start(f32[64,1536]{1,0:T(8,128)} %param.20) | copy-start | bytes 1179652
  63.1 96.4 %all-reduce.4.cloned.1.call-start = ((), (), s32[]{:S(2)}) async-start(), calls=%async_computation.6 | async-start | bytes 1310720 | tf_op jit(solution)/shard_map/psum | solution.py:51
  110.7 96.9 %all-gather.5.cloned.1.call-start = ((), (), s32[]{:S(2)}) async-start(), calls=%async_computation.3 | async-start | bytes 1310720 | tf_op jit(solution)/shard_map/all_gather | solution.py:70
  182.2 63.8 %all-gather.3.cloned.1.call-start = ((), (), s32[]{:S(2)}) async-start(), calls=%async_computation.2 | async-start | bytes 1966080 | tf_op jit(solution)/shard_map/all_gather | solution.py:66
  207.6 44.7 %copy-start.1 = (bf16[768,2048]{1,0:T(8,128)(2,1)S(1)}, bf16[768,2048]{1,0:T(8,128)(2,1)}, u32[]{:S(2)}) copy-start(bf16[768,2048]{1,0:T(8,128)(2,1)} %param.12) | copy-start | bytes 9437188
Sparse Core Ops, SparseCore 0:
  43.8 29.9 reduce-scatter.8
  76.7 33.9 reduce-scatter.6
  113.8 45.6 all-reduce.3
  182.4 25.2 all-gather.4
  209.6 36.3 all-gather.2
where the time goes:
time: 262 us; the launch traced here: 259 us
  waiting for transfers between devices  150 us (57%)
  matrix products  65.4 us (25%)
  blocking collectives  16.9 us (6%)
  between operations  15.6 us (6%)
  other arithmetic  6.95 us (3%)
  local copies, waits for them, and re-layouts  4.2 us (2%)
    psum x1, waiting for transfers between devices, on_device(): query_proj, out_proj = lax.psum((query_shard, out_shard), 'rep')  48.7 us
    reduce_scatter x1, waiting for transfers between devices, on_device(): lax.psum_scatter(query_early, 'fs', scatter_dimension=0, tiled=True)  36.9 us
    dot_general x2, matrix products, project(): lax.dot_general(basis.astype(jnp.float32), grad, (((0,), (0,)), ((), ()))...  34.6 us
    all_gather x1, waiting for transfers between devices, on_device(): lax.all_gather(query_dir, 'fs', axis=0, tiled=True)  30.8 us
    all_gather x1, waiting for transfers between devices, on_device(): lax.all_gather(out_dir, 'fs', axis=0, tiled=True)  22.7 us
    dot_general x2, matrix products, token_sum(): lax.dot_general(left, right, (((0,), (0,)), ((), ())), preferred_element_...  16.9 us
    psum x1, blocking collectives, on_device(): lax.psum((jnp.sum(query_proj * query_proj), jnp.sum(out_proj * out_proj))...  16.9 us
    reduce_scatter x1, waiting for transfers between devices, on_device(): lax.psum_scatter(out_early, 'fs', scatter_dimension=0, tiled=True)  10.7 us
  transfers between devices with their start and end apart: 5, of which 5 were waited for; matrix products, arithmetic and copies ran while one was open for 11% of the time, Pallas kernels for 0%

commit v1 on v0

--- a/solution.py
+++ b/solution.py
@@ -63,7 +63,9 @@
     out_left = out_local.astype(jnp.float32)
     query_step = jnp.dot(
         query_left,
-        lax.all_gather(query_dir, "fs", axis=0, tiled=True),
+        jnp.concatenate(
+            lax.all_to_all(jnp.stack([query_dir] * lax.axis_size("fs")), "fs", 0, 0), axis=0
+        ),
         precision=lax.Precision.HIGHEST,
     )
     out_step = jnp.dot(

time: 262 us -> 260 us (level)
  waiting for transfers between devices: 150 us -> 143 us
  starting transfers between devices: 0.2 us -> 4.51 us
    all_gather x1 -> x0, waiting for transfers between devices: 30.8 us -> none  [on_device(): lax.all_gather(query_dir, 'fs', axis=0, tiled=True)]
    all_gather x1, waiting for transfers between devices: 22.7 us -> 46.5 us  [on_device(): lax.all_gather(out_dir, 'fs', axis=0, tiled=True)]
    all_to_all x0 -> x1, starting transfers between devices: none -> 4.35 us  [on_device(): lax.all_to_all(jnp.stack([query_dir] * lax.axis_size('fs')), 'fs', 0, 0)]
  transfers between devices with their start and end apart: 5 -> 5, of which waited for: 5 -> 4; matrix products, arithmetic and copies ran while one was open for 11% -> 11% of each run, Pallas kernels for 0% -> 0%
where the time goes in v1:
time: 260 us; the launch traced here: 256 us
  waiting for transfers between devices  143 us (55%)
  matrix products  65.4 us (25%)
  blocking collectives  16.9 us (6%)
  between operations  15.6 us (6%)
  local copies, waits for them, and re-layouts  5.53 us (2%)
  other arithmetic  5.32 us (2%)
  starting transfers between devices  4.51 us (2%)
    psum x1, waiting for transfers between devices, on_device(): query_proj, out_proj = lax.psum((query_shard, out_shard), 'rep')  48.7 us
    all_gather x1, waiting for transfers between devices, on_device(): lax.all_gather(out_dir, 'fs', axis=0, tiled=True)  46.5 us
    reduce_scatter x1, waiting for transfers between devices, on_device(): lax.psum_scatter(query_early, 'fs', scatter_dimension=0, tiled=True)  36.9 us
    dot_general x2, matrix products, project(): lax.dot_general(basis.astype(jnp.float32), grad, (((0,), (0,)), ((), ()))...  34.6 us
    dot_general x2, matrix products, token_sum(): lax.dot_general(left, right, (((0,), (0,)), ((), ())), preferred_element_...  16.9 us
    psum x1, blocking collectives, on_device(): lax.psum((jnp.sum(query_proj * query_proj), jnp.sum(out_proj * out_proj))...  16.9 us
    reduce_scatter x1, waiting for transfers between devices, on_device(): lax.psum_scatter(out_early, 'fs', scatter_dimension=0, tiled=True)  10.7 us
    dot_general x1, matrix products, on_device(): jnp.dot(out_left, lax.all_gather(out_dir, 'fs', axis=0, tiled=True), prec...  7.46 us
  transfers between devices with their start and end apart: 5, of which 4 were waited for; matrix products, arithmetic and copies ran while one was open for 11% of the time, Pallas kernels for 0%

profile of v1, /device:TPU:0, one launch (start us, length us, event | category | flops | bytes accessed | tf_op | source)
XLA Modules:
  0.0 256.2 jit_solution(6766477965576251430)
XLA Ops:
  7.2 0.0 copy-start
  7.2 0.0 reduce-scatter.9.cloned.1.call-start
  7.2 0.0 copy-start.2
  7.2 9.9 %fusion.13 = f32[4096,1024]{1,0:T(8,128)S(1)} fusion(bf16[768,4096]{1,0:T(8,128)(2,1)} %param.14, bf16[768,1024]{1,0:T(8,128)(2,1)} %param.15), kind=kOutput, calls=%fused_computation.21 | convolution fusion | flops 6442450944 | bytes 24641536 | tf_op jit(solution)/shard_map/dot_general | solution.py:8
  17.1 0.0 copy-done.2
  17.1 24.0 %convolution_bitcast_fusion.1 = f32[256,1024]{0,1:T(8,128)} fusion(f32[4096,1024]{1,0:T(8,128)S(1)} %fusion.13, bf16[4096,256]{1,0:T(8,128)(2,1)S(1)} %copy-done.2), kind=kOutput, calls=%fused_computation.3 | convolution fusion | flops 12884901888 | bytes 19922944 | tf_op jit(solution)/shard_map/dot_general | solution.py:14
  41.2 2.5 copy.31
  43.7 0.0 reduce-scatter.9.cloned.1.call-update
  43.7 0.0 reduce-scatter.7.cloned.1.call-start
  43.8 0.0 copy-done
  43.8 0.0 copy-start.3
  43.8 7.0 %fusion.12 = f32[2048,1536]{1,0:T(8,128)S(1)} fusion(bf16[768,2048]{1,0:T(8,128)(2,1)S(1)} %copy-done, bf16[768,1536]{1,0:T(8,128)(2,1)} %param.13), kind=kOutput, calls=%fused_computation.20 | convolution fusion | flops 4831838208 | bytes 18087936 | tf_op jit(solution)/shard_map/dot_general | solution.py:8
  50.8 0.0 copy-done.3
  50.8 10.6 %convolution_bitcast_fusion = f32[256,1536]{0,1:T(8,128)S(1)} fusion(f32[2048,1536]{1,0:T(8,128)S(1)} %fusion.12, bf16[2048,256]{1,0:T(8,128)(2,1)S(1)} %copy-done.3), kind=kOutput, calls=%fused_computation.2 | convolution fusion | flops 9663676416 | bytes 15204352 | tf_op jit(solution)/shard_map/dot_general | solution.py:14
  61.4 0.0 copy-start.5
  61.4 0.0 copy-start.6
  61.4 1.6 copy.29
  63.1 0.0 reduce-scatter.7.cloned.1.call-update
  63.1 0.0 all-reduce.4.cloned.1.call-start
  63.1 10.7 %reduce-scatter.9.cloned.1.call-done = f32[64,1024]{1,0:T(8,128)} async-done(((f32[256,1024]{1,0:T(8,128)}), f32[64,1024]{1,0:T(8,128)}) %reduce-scatter.9.cloned.1.call-update) | async-done | bytes 262160 | tf_op jit(solution)/shard_map/reduce_scatter | solution.py:49
  73.9 36.9 %reduce-scatter.7.cloned.1.call-done = f32[64,1536]{1,0:T(8,128)} async-done(((f32[256,1536]{1,0:T(8,128)}), f32[64,1536]{1,0:T(8,128)}) %reduce-scatter.7.cloned.1.call-update) | async-done | bytes 393232 | tf_op jit(solution)/shard_map/reduce_scatter | solution.py:48
  110.7 0.0 all-reduce.4.cloned.1.call-update
  110.7 48.7 %all-reduce.4.cloned.1.call-done = (f32[64,1536]{1,0:T(8,128)}, f32[64,1024]{1,0:T(8,128)}) async-done(((f32[64,1536]{1,0:T(8,128)}, f32[64,1024]{1,0:T(8,128)}), (f32[64,1536]{1,0:T(8,128)}, f32[64,1024]{1,0:T(8,128)})) %all-reduce.4.cloned.1.call-update) | async-done | bytes 655376 | tf_op jit(solution)/shard_map/psum | solution.py:51
  159.5 1.7 multiply_reduce_fusion
  161.2 1.6 multiply_reduce_fusion.1
  162.8 16.9 %all-reduce = (f32[]{:T(128)}, f32[]{:T(128)}) all-reduce(f32[]{:T(128)} %multiply_reduce_fusion, f32[]{:T(128)} %multiply_reduce_fusion.1), channel_id=1, replica_groups=mesh['fs'=4,'rep'=4,'tp'=2] {'fs','tp'}, use_global_device_ids=true, to_apply=%region_3.0 | all-reduce | flops 2 | bytes 16 | tf_op jit(solution)/shard_map/psum | solution.py:52
  180.4 0.0 copy-done.5
  180.4 0.0 copy-done.6
  180.5 0.0 copy-start.4
  180.5 0.0 copy-start.7
  180.5 0.0 copy-start.8
  180.5 1.2 fusion.4
  181.7 1.3 stack.2
  183.0 4.3 %all-to-all-start = ((f32[4,64,1536]{2,1,0:T(8,128)}), f32[4,64,1536]{2,1,0:T(8,128)}, u32[]{:S(2)}, u32[]{:S(2)}) async-start(f32[4,64,1536]{2,1,0:T(8,128)} %stack.2), calls=%async_computation | async-start | bytes 3145728 | tf_op jit(solution)/shard_map/all_to_all | solution.py:67
  187.4 0.0 all-gather.2.cloned.1.call-start
  188.2 0.0 copy-done.4
  188.2 0.0 copy-done.7
  188.2 0.0 copy-done.8
  188.2 0.8 fusion.7
  189.0 0.0 all-gather.2.cloned.1.call-update
  189.0 46.5 %all-gather.2.cloned.1.call-done = f32[256,1024]{1,0:T(8,128)} async-done(((f32[64,1024]{1,0:T(8,128)}), f32[256,1024]{1,0:T(8,128)}) %all-gather.2.cloned.1.call-update) | async-done | bytes 1048592 | tf_op jit(solution)/shard_map/all_gather | solution.py:72
  235.5 7.5 %subtract_convert_fusion = (bf16[1024,1024]{1,0:T(8,128)(2,1)}, f32[1024,1024]{1,0:T(8,128)}) fusion(f32[1024,1024]{1,0:T(8,128)} %param.17, f32[256,1024]{1,0:T(8,128)} %all-gather.2.cloned.1.call-done, bf16[4096,256]{1,0:T(8,128)(2,1)} %param.19, s32[]{:T(128)S(6)} %select_n.7), kind=kOutput, calls=%fused_computation | convolution fusion | flops 3224371200 | bytes 12058628 | tf_op jit(solution)/shard_map/dot_general | solution.py:71
  243.0 0.0 all-to-all-done
  243.0 0.0 copy-start.1
  243.0 6.4 %subtract_convert_fusion.1 = (bf16[512,1536]{1,0:T(8,128)(2,1)}, f32[512,1536]{1,0:T(8,128)}) fusion(f32[512,1536]{1,0:T(8,128)} %param.16, f32[256,1536]{1,0:T(8,128)} %bitcast.1, bf16[2048,256]{1,0:T(8,128)(2,1)} %param.18, s32[]{:T(128)S(6)} %select_n.6), kind=kOutput, calls=%fused_computation.1 | convolution fusion | flops 2418278400 | bytes 9699332 | tf_op jit(solution)/shard_map/dot_general | solution.py:64
  249.4 0.0 copy-done.1
Async XLA Ops:
  7.2 36.6 %copy-start = (bf16[768,2048]{1,0:T(8,128)(2,1)S(1)}, bf16[768,2048]{1,0:T(8,128)(2,1)}, u32[]{:S(2)}) copy-start(bf16[768,2048]{1,0:T(8,128)(2,1)} %param.12) | copy-start | bytes 9437188
  7.2 66.7 %reduce-scatter.9.cloned.1.call-start = ((), (), s32[]{:S(2)}) async-start(), calls=%async_computation.5 | async-start | bytes 1310720 | tf_op jit(solution)/shard_map/reduce_scatter | solution.py:49
  7.2 9.9 %copy-start.2 = (bf16[4096,256]{1,0:T(8,128)(2,1)S(1)}, bf16[4096,256]{1,0:T(8,128)(2,1)}, u32[]{:S(2)}) copy-start(bf16[4096,256]{1,0:T(8,128)(2,1)} %param.19) | copy-start | bytes 6291460
  43.7 67.0 %reduce-scatter.7.cloned.1.call-start = ((), (), s32[]{:S(2)}) async-start(), calls=%async_computation.4 | async-start | bytes 1966080 | tf_op jit(solution)/shard_map/reduce_scatter | solution.py:48
  43.8 7.1 %copy-start.3 = (bf16[2048,256]{1,0:T(8,128)(2,1)S(1)}, bf16[2048,256]{1,0:T(8,128)(2,1)}, u32[]{:S(2)}) copy-start(bf16[2048,256]{1,0:T(8,128)(2,1)} %param.18) | copy-start | bytes 3145732
  61.4 119.0 %copy-start.5 = (f32[64,1536]{1,0:T(8,128)S(1)}, f32[64,1536]{1,0:T(8,128)}, u32[]{:S(2)}) copy-start(f32[64,1536]{1,0:T(8,128)} %param.21) | copy-start | bytes 1179652
  61.4 119.0 %copy-start.6 = (f32[64,1536]{1,0:T(8,128)S(1)}, f32[64,1536]{1,0:T(8,128)}, u32[]{:S(2)}) copy-start(f32[64,1536]{1,0:T(8,128)} %param.20) | copy-start | bytes 1179652
  63.1 96.4 %all-reduce.4.cloned.1.call-start = ((), (), s32[]{:S(2)}) async-start(), calls=%async_computation.6 | async-start | bytes 1310720 | tf_op jit(solution)/shard_map/psum | solution.py:51
  180.5 7.7 %copy-start.4 = (f32[64,1024]{1,0:T(8,128)S(1)}, f32[64,1024]{1,0:T(8,128)}, u32[]{:S(2)}) copy-start(f32[64,1024]{1,0:T(8,128)} %get-tuple-element.7) | copy-start | bytes 786436
  180.5 7.7 %copy-start.7 = (f32[64,1024]{1,0:T(8,128)S(1)}, f32[64,1024]{1,0:T(8,128)}, u32[]{:S(2)}) copy-start(f32[64,1024]{1,0:T(8,128)} %param.23) | copy-start | bytes 786436
  180.5 7.7 %copy-start.8 = (f32[64,1024]{1,0:T(8,128)S(1)}, f32[64,1024]{1,0:T(8,128)}, u32[]{:S(2)}) copy-start(f32[64,1024]{1,0:T(8,128)} %param.22) | copy-start | bytes 786436
  183.0 60.0 %all-to-all-start = ((f32[4,64,1536]{2,1,0:T(8,128)}), f32[4,64,1536]{2,1,0:T(8,128)}, u32[]{:S(2)}, u32[]{:S(2)}) async-start(f32[4,64,1536]{2,1,0:T(8,128)} %stack.2), calls=%async_computation | async-start | bytes 3145728 | tf_op jit(solution)/shard_map/all_to_all | solution.py:67
  187.4 48.1 %all-gather.2.cloned.1.call-start = ((), (), s32[]{:S(2)}) async-start(), calls=%async_computation.3 | async-start | bytes 1310720 | tf_op jit(solution)/shard_map/all_gather | solution.py:72
  243.0 6.4 %copy-start.1 = (bf16[768,2048]{1,0:T(8,128)(2,1)S(1)}, bf16[768,2048]{1,0:T(8,128)(2,1)}, u32[]{:S(2)}) copy-start(bf16[768,2048]{1,0:T(8,128)(2,1)} %param.12) | copy-start | bytes 9437188
Sparse Core Ops, SparseCore 0:
  43.8 29.9 reduce-scatter.8
  76.7 33.9 reduce-scatter.6
  113.8 45.6 all-reduce.3
  190.0 45.4 all-gather.1
